TPU v7x, 256 devices: a whole 4x4x8 slice. The times are simulated.
256 devices in a mesh: ep: 128 (over z, y, x), tp: 2 (over core).
Axes of the slice: x: 4, y: 4, z: 8, core: 2. Of those that a mesh axis runs over, the one named last changes fastest.
Arguments:
- tokens: bfloat16 [2048, 2048], P('ep', 'tp'), may hold values from -6 to 6
- lengths: int32 [2048], P('ep'), may hold values from 1 to 1024
- lat_cache: bfloat16 [2048, 1024, 256], P(('ep', 'tp')), may hold values from -6 to 6
- rope_cache: bfloat16 [2048, 1024, 32], P(('ep', 'tp'))
- norm1_gain: float32 [2048], replicated, may hold values from 0.1 to 1.9
- w_qdown: bfloat16 [2048, 512], P('tp'), may hold values from -0.125 to 0.125
- w_kvdown: bfloat16 [2048, 256], P('tp'), may hold values from -0.125 to 0.125
- w_kdown_rope: bfloat16 [2048, 32], P('tp'), may hold values from -0.125 to 0.125
- qnorm_gain: float32 [512], replicated, may hold values from 0.1 to 1.9
- kvnorm_gain: float32 [256], replicated, may hold values from 0.1 to 1.9
- w_qup_nope: bfloat16 [512, 16, 64], P(None, 'tp'), may hold values from -0.25 to 0.25
- w_qup_rope: bfloat16 [512, 16, 32], P(None, 'tp'), may hold values from -0.25 to 0.25
- w_absorb_k: bfloat16 [16, 64, 256], P('tp'), may hold values from -0.75 to 0.75
- w_absorb_v: bfloat16 [16, 256, 64], P('tp'), may hold values from -0.375 to 0.375
- w_attn_out: bfloat16 [16, 64, 2048], P('tp'), may hold values from -0.1875 to 0.1875
- norm2_gain: float32 [2048], replicated, may hold values from 0.1 to 1.9
- routes: int32 [2048, 6], P('ep'), may hold values from 0 to 127, all different within a row; in each aligned block of 16 rows (0 to 15, 16 to 31, ...) at most 2 rows name the same one
- route_weights: float32 [2048, 6], P('ep'), may hold values from 0.1 to 1
- w_exp_gate: bfloat16 [128, 2048, 512], P('ep', None, 'tp'), may hold values from -0.125 to 0.125
- w_exp_up: bfloat16 [128, 2048, 512], P('ep', None, 'tp'), may hold values from -0.125 to 0.125
- w_exp_down: bfloat16 [128, 512, 2048], P('ep', 'tp'), may hold values from -0.25 to 0.25
Outputs:
- mixed: bfloat16 [2048, 2048], P('ep', 'tp')
- new_latent: bfloat16 [2048, 256], P(('ep', 'tp'))
- new_rope_key: bfloat16 [2048, 32], P(('ep', 'tp'))
Inputs may be any that keep to these rules, and one draw needn't show every extreme that they name: `routes`: each row names 6 different experts; the 16 rows of one index of ep name one expert at most 2 times, and some expert exactly so often. `lengths`: the new token's position; cached positions from it on are not in use.
All inputs are finite; a program needn't handle non-finite values.
Results may differ from a plain program's by a relative error of at most 0.015.
Values may be sent and summed in bfloat16 or wider, within the bound.
A program may use at most 64 MiB of HBM per device.

v0:
```python
import jax
import jax.numpy as jnp
from jax import lax
from jax.sharding import PartitionSpec as P

rms_eps = 1e-06
rope_base = 10000.0


def laid_out(blocks, dim):
    shape = list(blocks.shape[1:])
    shape[dim] *= blocks.shape[0]
    return jnp.moveaxis(blocks, 0, dim).reshape(shape)


def from_everyone(array, axis):
    size = lax.axis_size(axis)
    return lax.all_to_all(
        jnp.broadcast_to(array[None], (size, *array.shape)), axis, 0, 0, tiled=True
    )


def gather_directly(array, axis, dim):
    return laid_out(from_everyone(array, axis), dim)


def over_copies(array, axis):
    everything = from_everyone(array, axis)
    return jnp.sum(everything, axis=0)


def in_one(arrays, axis):
    vector, at, outs = (jnp.concatenate([a.reshape(-1) for a in arrays]), 0, [])
    running = over_copies(vector, axis)
    for a in arrays:
        outs.append(running[at : at + a.size].reshape(a.shape))
        at += a.size
    return tuple(outs)


def sent_together(arrays, axis, split_dim, concat_dim, along):
    ends, at = ([], 0)
    for a in arrays[:-1]:
        at += a.shape[along]
        ends.append(at)
    both = jnp.concatenate(arrays, axis=along)
    return tuple(
        jnp.split(
            lax.all_to_all(both, axis, split_axis=split_dim, concat_axis=concat_dim, tiled=True),
            ends,
            axis=along,
        )
    )


def cut_along(array, dim, size):
    before, after = (array.shape[:dim], array.shape[dim + 1 :])
    return jnp.moveaxis(array.reshape(*before, size, -1, *after), dim, 0)


def summed_on_arrival(array, axis, dim):
    size = lax.axis_size(axis)
    blocks = lax.all_to_all(cut_along(array, dim, size), axis, 0, 0, tiled=True)
    return jnp.sum(blocks, axis=0)


def rms_scale(values, gain_vector):
    mean_square = jnp.mean(values * values, axis=-1, keepdims=True)
    return values * lax.rsqrt(mean_square + rms_eps) * gain_vector


def rotate(values, positions):
    half_size = values.shape[-1] // 2
    frequency = jnp.exp(-jnp.log(rope_base) * jnp.arange(half_size, dtype=jnp.float32) / half_size)
    angles = positions.astype(jnp.float32)[:, None] * frequency[None, :]
    view_shape = (angles.shape[0],) + (1,) * (values.ndim - 2) + (half_size,)
    cosine = jnp.cos(angles).reshape(view_shape)
    sine_part = jnp.sin(angles).reshape(view_shape)
    first_half = values[..., :half_size]
    second_half = values[..., half_size:]
    return jnp.concatenate(
        [
            first_half * cosine - second_half * sine_part,
            second_half * cosine + first_half * sine_part,
        ],
        -1,
    )


def slot_tables(group_routes, group_weights, experts, capacity):
    row_count, top_count = group_routes.shape
    flat_routes = group_routes.reshape(-1)
    matches = (flat_routes[:, None] == jnp.arange(experts, dtype=jnp.int32)[None, :]).astype(
        jnp.int32
    )
    earlier = jnp.cumsum(matches, axis=0) - matches
    slot_index = jnp.sum(earlier * matches, axis=1)
    target = flat_routes * capacity + slot_index
    slot_match = (
        target[:, None] == jnp.arange(experts * capacity, dtype=jnp.int32)[None, :]
    ).astype(jnp.float32)
    slot_match = slot_match.reshape(row_count, top_count, experts * capacity)
    dispatch = jnp.sum(slot_match, axis=1).T
    weighing = jnp.sum(slot_match * group_weights[:, :, None], axis=1)
    return (dispatch, weighing)


def attend(query_latent, query_rope, latents, rope_keys, fresh_latent, fresh_rope, own_lengths):
    past_scores = jnp.einsum(
        "shc,spc->shp", query_latent, latents, preferred_element_type=jnp.float32
    )
    past_scores = past_scores + jnp.einsum(
        "shr,spr->shp", query_rope, rope_keys, preferred_element_type=jnp.float32
    )
    cache_positions = lax.broadcasted_iota(jnp.int32, past_scores.shape, 2)
    past_scores = jnp.where(cache_positions < own_lengths[:, None, None], past_scores, -jnp.inf)
    own_score = jnp.einsum(
        "shc,sc->sh", query_latent, fresh_latent, preferred_element_type=jnp.float32
    )
    own_score = own_score + jnp.einsum(
        "shr,sr->sh", query_rope, fresh_rope, preferred_element_type=jnp.float32
    )
    row_peak = jnp.maximum(jnp.max(past_scores, axis=2), own_score)
    past_weights = jnp.exp(past_scores - row_peak[:, :, None])
    own_weight = jnp.exp(own_score - row_peak)
    denominator = jnp.sum(past_weights, axis=2) + own_weight
    past_probs = (past_weights / denominator[:, :, None]).astype(jnp.bfloat16)
    own_prob = (own_weight / denominator).astype(jnp.bfloat16)
    mixed_latent = jnp.einsum(
        "shp,spc->shc", past_probs, latents, preferred_element_type=jnp.float32
    )
    mixed_latent = (
        mixed_latent
        + own_prob.astype(jnp.float32)[:, :, None] * fresh_latent.astype(jnp.float32)[:, None, :]
    )
    return mixed_latent.astype(jnp.bfloat16)


def expert_pass(expert_rows, w_exp_gate, w_exp_up, w_exp_down):
    gate_value = jnp.einsum(
        "gecd,edh->gech", expert_rows, w_exp_gate, preferred_element_type=jnp.float32
    )
    up_value = jnp.einsum(
        "gecd,edh->gech", expert_rows, w_exp_up, preferred_element_type=jnp.float32
    )
    expert_hidden = (jax.nn.silu(gate_value) * up_value).astype(jnp.bfloat16)
    return jnp.einsum(
        "gech,ehd->gecd", expert_hidden, w_exp_down, preferred_element_type=jnp.float32
    )


def local(
    tokens,
    lengths,
    lat_cache,
    rope_cache,
    norm1_gain,
    w_qdown,
    w_kvdown,
    w_kdown_rope,
    qnorm_gain,
    kvnorm_gain,
    w_qup_nope,
    w_qup_rope,
    w_absorb_k,
    w_absorb_v,
    w_attn_out,
    norm2_gain,
    routes,
    route_weights,
    w_exp_gate,
    w_exp_up,
    w_exp_down,
):
    score_scale = (w_qup_nope.shape[2] + w_qup_rope.shape[2]) ** (-0.5)
    core_index = lax.axis_index("tp")
    group_rows = tokens.shape[0]
    own_rows = lat_cache.shape[0]
    full_tokens = gather_directly(tokens, "tp", 1)
    token_values = full_tokens.astype(jnp.float32)
    model_width = full_tokens.shape[1]
    half_width = tokens.shape[1]
    normed1 = rms_scale(token_values, norm1_gain).astype(jnp.bfloat16)
    feature_rows = w_qdown.shape[0]
    local_rows = lax.dynamic_slice_in_dim(normed1, core_index * feature_rows, feature_rows, 1)
    query_low, kv_low, rope_low = in_one(
        (
            jnp.dot(local_rows, w_qdown, preferred_element_type=jnp.float32),
            jnp.dot(local_rows, w_kvdown, preferred_element_type=jnp.float32),
            jnp.dot(local_rows, w_kdown_rope, preferred_element_type=jnp.float32),
        ),
        "tp",
    )
    compressed = rms_scale(query_low, qnorm_gain).astype(jnp.bfloat16)
    latent_all = rms_scale(kv_low, kvnorm_gain).astype(jnp.bfloat16)
    rope_all = rotate(rope_low, lengths).astype(jnp.bfloat16)
    query_nope = jnp.einsum(
        "sc,chd->shd", compressed, w_qup_nope, preferred_element_type=jnp.float32
    ).astype(jnp.bfloat16)
    rope_part = jnp.einsum(
        "sc,chd->shd", compressed, w_qup_rope, preferred_element_type=jnp.float32
    )
    query_rope = (rotate(rope_part, lengths) * score_scale).astype(jnp.bfloat16)
    query_latent = (
        jnp.einsum("shd,hdc->shc", query_nope, w_absorb_k, preferred_element_type=jnp.float32)
        * score_scale
    ).astype(jnp.bfloat16)
    seq_latent, seq_rope = sent_together((query_latent, query_rope), "tp", 0, 1, 2)
    first_row = core_index * own_rows
    new_latent = lax.dynamic_slice_in_dim(latent_all, first_row, own_rows, 0)
    new_rope_key = lax.dynamic_slice_in_dim(rope_all, first_row, own_rows, 0)
    own_lengths = lax.dynamic_slice_in_dim(lengths, first_row, own_rows, 0)
    attended = attend(
        seq_latent, seq_rope, lat_cache, rope_cache, new_latent, new_rope_key, own_lengths
    )
    head_latent = lax.all_to_all(attended, "tp", split_axis=1, concat_axis=0, tiled=True)
    head_out = jnp.einsum(
        "shc,hcv->shv", head_latent, w_absorb_v, preferred_element_type=jnp.float32
    ).astype(jnp.bfloat16)
    attention_sum = over_copies(
        jnp.einsum("shv,hvd->sd", head_out, w_attn_out, preferred_element_type=jnp.float32), "tp"
    )
    hidden1 = (token_values + attention_sum).astype(jnp.bfloat16)
    normed2 = rms_scale(hidden1.astype(jnp.float32), norm2_gain).astype(jnp.bfloat16)
    own_half = lax.dynamic_slice_in_dim(hidden1, core_index * half_width, half_width, 1).astype(
        jnp.float32
    )
    groups = lax.axis_size("ep")
    experts_here = w_exp_gate.shape[0]
    total_experts = groups * experts_here
    top_count = routes.shape[1]
    capacity = max(2, group_rows * top_count * 8 // 3 // total_experts)
    dispatch, weighing = slot_tables(routes, route_weights, total_experts, capacity)
    sent_rows = jnp.dot(
        dispatch.astype(jnp.bfloat16), normed2, preferred_element_type=jnp.float32
    ).astype(jnp.bfloat16)
    sent_rows = sent_rows.reshape(groups, experts_here, capacity, model_width)
    partial_out = expert_pass(
        lax.all_to_all(sent_rows, "ep", split_axis=0, concat_axis=0, tiled=True),
        w_exp_gate,
        w_exp_up,
        w_exp_down,
    )
    summed = summed_on_arrival(partial_out, "tp", 3).astype(jnp.bfloat16)
    returned = lax.all_to_all(summed, "ep", split_axis=0, concat_axis=0, tiled=True)
    routed = jnp.dot(
        weighing, returned.reshape(total_experts * capacity, half_width).astype(jnp.float32)
    )
    mixed = (own_half + routed).astype(jnp.bfloat16)
    return (mixed, new_latent, new_rope_key)


def solution(mesh):
    return jax.shard_map(
        local,
        mesh=mesh,
        in_specs=(
            P("ep", "tp"),
            P("ep"),
            P(("ep", "tp"), None, None),
            P(("ep", "tp"), None, None),
            P(),
            P("tp", None),
            P("tp", None),
            P("tp", None),
            P(),
            P(),
            P(None, "tp", None),
            P(None, "tp", None),
            P("tp", None, None),
            P("tp", None, None),
            P("tp", None, None),
            P(),
            P("ep", None),
            P("ep", None),
            P("ep", None, "tp"),
            P("ep", None, "tp"),
            P("ep", "tp", None),
        ),
        out_specs=(P("ep", "tp"), P(("ep", "tp"), None), P(("ep", "tp"), None)),
        check_vma=False,
    )
```

profile of v0, /device:TPU:1, one launch (start us, length us, event | category | flops | bytes accessed | tf_op | source)
XLA Modules:
  0.0 131.3 jit_solution(5113746206618433155)
XLA Ops:
  0.7 1.5 %broadcast_in_dim.9 = bf16[2,16,1024]{2,1,0:T(8,128)(2,1)} broadcast(bf16[16,1024]{1,0:T(8,128)(2,1)} %param.21), dimensions={1,2} | broadcast | bytes 98304 | tf_op jit(solution)/shard_map/broadcast_in_dim | solution.py:19
  2.2 6.5 %all-to-all-start = ((bf16[2,16,1024]{2,1,0:T(8,128)(2,1)}), bf16[2,16,1024]{2,1,0:T(8,128)(2,1)S(1)}, u32[]{:S(2)}, u32[]{:S(2)}) async-start(bf16[2,16,1024]{2,1,0:T(8,128)(2,1)} %broadcast_in_dim.9), calls=%async_computation | async-start | bytes 131072 | tf_op jit(solution)/shard_map/all_to_all | solution.py:18
  8.7 1.1 all-to-all-done
  10.0 0.7 dynamic-slice
  10.8 1.0 fusion.67
  11.8 1.2 convolution_bitcast_fusion.4
  13.1 1.5 %convolution_bitcast_fusion.3 = f32[2,4,8,128]{3,2,1,0:T(8,128)S(1)} fusion(bf16[16,1024]{1,0:T(8,128)(2,1)S(1)} %fusion.35, bf16[1024,512]{1,0:T(8,128)(2,1)} %param.26), kind=kOutput, calls=%fused_computation.20 | convolution fusion | flops 16777216 | bytes 1114112 | tf_op jit(solution)/shard_map/dot_general | solution.py:188
  15.3 3.7 %all-to-all-start.1 = ((f32[2,1,12800]{2,1,0:T(1,128)}), f32[2,1,12800]{2,1,0:T(1,128)S(1)}, u32[]{:S(2)}, u32[]{:S(2)}) async-start(f32[2,1,12800]{2,1,0:T(1,128)} %broadcast_in_dim.10), calls=%async_computation.1 | async-start | bytes 204800 | tf_op jit(solution)/shard_map/all_to_all | solution.py:18
  19.0 1.1 all-to-all-done.1
  22.3 3.7 %all-to-all-start.2 = ((bf16[16,8,288]{2,1,0:T(8,128)(2,1)}), bf16[16,8,288]{2,1,0:T(8,128)(2,1)S(1)}, u32[]{:S(2)}, u32[]{:S(2)}) async-start(bf16[16,8,288]{2,1,0:T(8,128)(2,1)} %copy.100), calls=%async_computation.2 | async-start | bytes 196608 | tf_op jit(solution)/shard_map/all_to_all | solution.py:49
  26.2 0.8 all-to-all-done.2
  27.5 3.5 %fusion.43 = f32[8,16,1024]{2,1,0:T(8,128)S(1)} fusion(bf16[8,1024,256]{2,1,0:T(8,128)(2,1)} %param.23, bf16[8,16,288]{2,1,0:T(8,128)(2,1)S(1)} %bitcast.142), kind=kOutput, calls=%fused_computation.69 | convolution fusion | flops 67108864 | bytes 4784128 | tf_op jit(solution)/shard_map/shc,spc->shp/dot_general | solution.py:109
  31.6 0.7 fusion.5
  32.4 3.8 %all_to_all.67 = bf16[8,16,256]{2,0,1:T(8,128)(2,1)S(1)} all-to-all(bf16[8,16,256]{2,0,1:T(8,128)(2,1)S(1)} %copy.102), channel_id=1, replica_groups=mesh['ep'=128,'tp'=2] {'tp'}, dimensions={1} | all-to-all | bytes 131072 | tf_op jit(solution)/shard_map/all_to_all | solution.py:216
  36.8 0.7 broadcast_in_dim.12
  37.5 3.8 %all-to-all-start.4 = ((f32[2,16,2048]{2,1,0:T(8,128)}), f32[2,16,2048]{2,1,0:T(8,128)S(1)}, u32[]{:S(2)}, u32[]{:S(2)}) async-start(f32[2,16,2048]{2,1,0:T(8,128)} %broadcast_in_dim.12), calls=%async_computation.4 | async-start | bytes 524288 | tf_op jit(solution)/shard_map/all_to_all | solution.py:18
  43.3 1.5 %reshape.211 = bf16[128,1,2,2048]{3,2,0,1:T(2,128)(2,1)} reshape(bf16[256,2048]{1,0:T(8,128)(2,1)S(1)} %convolution_convert_fusion) | data formatting | bytes 2097152 | tf_op jit(solution)/shard_map/reshape | solution.py:237
  44.8 43.1 %all_to_all.68 = bf16[128,1,2,2048]{3,2,1,0:T(2,128)(2,1)S(1)} all-to-all(bf16[128,1,2,2048]{3,2,1,0:T(2,128)(2,1)} %bitcast.135), channel_id=1, replica_groups=mesh['ep'=128,'tp'=2] {'ep'}, dimensions={0} | all-to-all | bytes 2097152 | tf_op jit(solution)/shard_map/all_to_all | solution.py:239
  88.6 4.2 %fusion.9 = f32[128,2,2048]{2,0,1:T(8,128)} fusion(bf16[1,256,2048]{2,1,0:T(8,128)(2,1)} %param.41, bf16[1,2048,256]{2,1,0:T(8,128)(2,1)} %param.40, bf16[128,1,2,2048]{3,2,1,0:T(2,128)(2,1)S(1)} %all_to_all.68, f32[128,1,2,256]{3,0,2,1:T(8,128)S(1)} %convolution_bitcast_fusion.2), kind=kOutput, calls=%fused_computation.22 | convolution fusion | flops 537264128 | bytes 5505024 | tf_op jit(solution)/shard_map/gech,ehd->gecd/dot_general | solution.py:147
  92.8 1.7 %copy.151 = f32[1,2,16,2,8,1024]{5,4,2,1,0,3:T(8,128)S(1)} copy(f32[1,2,16,2,8,1024]{5,4,3,2,1,0:T(8,128)} %bitcast.133) | data formatting | bytes 4194304 | tf_op jit(solution)/shard_map/reshape | solution.py:58
  94.5 9.0 %all_to_all.69 = f32[2,128,1,2,1024]{4,1,3,2,0:T(8,128)} all-to-all(f32[2,128,1,2,1024]{4,1,3,2,0:T(8,128)S(1)} %bitcast.134), channel_id=1, replica_groups=mesh['ep'=128,'tp'=2] {'tp'}, dimensions={0} | all-to-all | bytes 4194304 | tf_op jit(solution)/shard_map/all_to_all | solution.py:63
  103.5 1.8 %reduce_sum.115 = bf16[128,2,1024]{2,0,1:T(8,128)(2,1)S(1)} reduce(f32[2,128,1,2,1024]{4,1,3,2,0:T(8,128)} %all_to_all.69, f32[]{:T(128)} %constant.20.clone.1), dimensions={0,2}, to_apply=%region_12.13 | reduce | flops 262144 | bytes 2621444 | tf_op jit(solution)/shard_map/reduce_sum | solution.py:64
  105.8 24.4 %all_to_all.70 = bf16[128,1,2,1024]{3,2,1,0:T(2,128)(2,1)S(1)} all-to-all(bf16[128,1,2,1024]{3,2,1,0:T(2,128)(2,1)S(1)} %copy.113), channel_id=1, replica_groups=mesh['ep'=128,'tp'=2] {'ep'}, dimensions={0} | all-to-all | bytes 1048576 | tf_op jit(solution)/shard_map/all_to_all | solution.py:245
  130.5 0.8 fusion.7
  (94 shorter events, 8.4 us)
Async XLA Ops:
  0.6 35.5 %copy-start = (bf16[8,64,2048]{2,1,0:T(8,128)(2,1)S(1)}, bf16[8,64,2048]{2,1,0:T(8,128)(2,1)}, u32[]{:S(2)}) copy-start(bf16[8,64,2048]{2,1,0:T(8,128)(2,1)} %param.35) | copy-start | bytes 6291460
  0.6 19.6 %copy-start.15 = (s32[16]{0:T(128)S(1)}, s32[16]{0:T(128)}, u32[]{:S(2)}) copy-start(s32[16]{0:T(128)} %param.22) | copy-start | bytes 196
  0.7 19.8 %copy-start.9 = (f32[512]{0:T(512)S(1)}, f32[512]{0:T(512)}, u32[]{:S(2)}) copy-start(f32[512]{0:T(512)} %param.29) | copy-start | bytes 6148
  0.7 20.1 %copy-start.4 = (bf16[8,64,256]{2,1,0:T(8,128)(2,1)S(1)}, bf16[8,64,256]{2,1,0:T(8,128)(2,1)}, u32[]{:S(2)}) copy-start(bf16[8,64,256]{2,1,0:T(8,128)(2,1)} %param.33) | copy-start | bytes 786436
  0.7 20.1 %copy-start.2 = (bf16[512,8,64]{0,2,1:T(8,128)(2,1)S(1)}, bf16[512,8,64]{0,2,1:T(8,128)(2,1)}, u32[]{:S(2)}) copy-start(bf16[512,8,64]{0,2,1:T(8,128)(2,1)} %param.31) | copy-start | bytes 1572868
  2.2 7.6 %all-to-all-start = ((bf16[2,16,1024]{2,1,0:T(8,128)(2,1)}), bf16[2,16,1024]{2,1,0:T(8,128)(2,1)S(1)}, u32[]{:S(2)}, u32[]{:S(2)}) async-start(bf16[2,16,1024]{2,1,0:T(8,128)(2,1)} %broadcast_in_dim.9), calls=%async_computation | async-start | bytes 131072 | tf_op jit(solution)/shard_map/all_to_all | solution.py:18
  10.0 10.5 %copy-start.6 = (bf16[512,8,32]{0,2,1:T(8,128)(2,1)S(1)}, bf16[512,8,32]{0,2,1:T(8,128)(2,1)}, u32[]{:S(2)}) copy-start(bf16[512,8,32]{0,2,1:T(8,128)(2,1)} %param.32) | copy-start | bytes 786436
  13.1 14.1 %copy-start.13 = (f32[256]{0:T(256)S(1)}, f32[256]{0:T(256)}, u32[]{:S(2)}) copy-start(f32[256]{0:T(256)} %param.30) | copy-start | bytes 3076
  15.3 4.8 %all-to-all-start.1 = ((f32[2,1,12800]{2,1,0:T(1,128)}), f32[2,1,12800]{2,1,0:T(1,128)S(1)}, u32[]{:S(2)}, u32[]{:S(2)}) async-start(f32[2,1,12800]{2,1,0:T(1,128)} %broadcast_in_dim.10), calls=%async_computation.1 | async-start | bytes 204800 | tf_op jit(solution)/shard_map/all_to_all | solution.py:18
  22.3 4.8 %all-to-all-start.2 = ((bf16[16,8,288]{2,1,0:T(8,128)(2,1)}), bf16[16,8,288]{2,1,0:T(8,128)(2,1)S(1)}, u32[]{:S(2)}, u32[]{:S(2)}) async-start(bf16[16,8,288]{2,1,0:T(8,128)(2,1)} %copy.100), calls=%async_computation.2 | async-start | bytes 196608 | tf_op jit(solution)/shard_map/all_to_all | solution.py:49
  27.1 3.9 %copy-start.12 = (bf16[8,32]{1,0:T(8,128)(2,1)}, bf16[8,32]{1,0:T(8,128)(2,1)S(1)}, u32[]{:S(2)}) copy-start(bf16[8,32]{1,0:T(8,128)(2,1)S(1)} %fusion.56) | copy-start | bytes 1540
  27.2 3.8 %copy-start.11 = (bf16[8,256]{1,0:T(8,128)(2,1)}, bf16[8,256]{1,0:T(8,128)(2,1)S(1)}, u32[]{:S(2)}) copy-start(bf16[8,256]{1,0:T(8,128)(2,1)S(1)} %get-tuple-element.6) | copy-start | bytes 12292
  27.5 3.6 %copy-start.3 = (bf16[8,1024,32]{1,2,0:T(8,128)(2,1)S(1)}, bf16[8,1024,32]{1,2,0:T(8,128)(2,1)}, u32[]{:S(2)}) copy-start(bf16[8,1024,32]{1,2,0:T(8,128)(2,1)} %param.24) | copy-start | bytes 1572868
  27.5 4.1 %copy-start.1 = (bf16[8,1024,256]{2,1,0:T(8,128)(2,1)S(1)}, bf16[8,1024,256]{2,1,0:T(8,128)(2,1)}, u32[]{:S(2)}) copy-start(bf16[8,1024,256]{2,1,0:T(8,128)(2,1)} %param.23) | copy-start | bytes 12582916
  31.6 4.6 %copy-start.5 = (bf16[8,256,64]{1,2,0:T(8,128)(2,1)S(1)}, bf16[8,256,64]{1,2,0:T(8,128)(2,1)}, u32[]{:S(2)}) copy-start(bf16[8,256,64]{1,2,0:T(8,128)(2,1)} %param.34) | copy-start | bytes 786436
  32.3 9.0 %copy-start.7 = (s32[16,6]{0,1:T(8,128)S(1)}, s32[16,6]{0,1:T(8,128)}, u32[]{:S(2)}) copy-start(s32[16,6]{0,1:T(8,128)} %param.37) | copy-start | bytes 1156
  36.2 6.5 %copy-start.10 = (f32[16,6]{0,1:T(8,128)S(1)}, f32[16,6]{0,1:T(8,128)}, u32[]{:S(2)}) copy-start(f32[16,6]{0,1:T(8,128)} %param.38) | copy-start | bytes 1156
  36.2 6.6 %copy-start.8 = (f32[2048]{0:T(1024)S(1)}, f32[2048]{0:T(1024)}, u32[]{:S(2)}) copy-start(f32[2048]{0:T(1024)} %param.36) | copy-start | bytes 24580
  37.5 5.0 %all-to-all-start.4 = ((f32[2,16,2048]{2,1,0:T(8,128)}), f32[2,16,2048]{2,1,0:T(8,128)S(1)}, u32[]{:S(2)}, u32[]{:S(2)}) async-start(f32[2,16,2048]{2,1,0:T(8,128)} %broadcast_in_dim.12), calls=%async_computation.4 | async-start | bytes 524288 | tf_op jit(solution)/shard_map/all_to_all | solution.py:18
  44.8 43.1 %copy-start.14 = (bf16[1,2048,256]{2,1,0:T(8,128)(2,1)S(1)}, bf16[1,2048,256]{2,1,0:T(8,128)(2,1)}, u32[]{:S(2)}) copy-start(bf16[1,2048,256]{2,1,0:T(8,128)(2,1)} %param.39) | copy-start | bytes 3145732
where the time goes:
time: 133 us; the launch traced here: 131 us
  blocking collectives  80.3 us (60%)
  starting transfers between devices  17.6 us (13%)
  matrix products  16 us (12%)
  local copies, waits for them, and re-layouts  9.15 us (7%)
  other arithmetic  3.85 us (3%)
  waiting for transfers between devices  3.4 us (3%)
    all_to_all x1, blocking collectives, local(): lax.all_to_all(sent_rows, 'ep', split_axis=0, concat_axis=0, tiled=True)  43.1 us
    all_to_all x1, blocking collectives, local(): lax.all_to_all(summed, 'ep', split_axis=0, concat_axis=0, tiled=True)  24.4 us
    all_to_all x3, starting transfers between devices, from_everyone(): lax.all_to_all(jnp.broadcast_to(array[None], (size, *array.shape)), axis,...  13.9 us
    all_to_all x1, blocking collectives, summed_on_arrival(): blocks = lax.all_to_all(cut_along(array, dim, size), axis, 0, 0, tiled=True)  8.99 us
    dot_general x1, matrix products, expert_pass(): jnp.einsum('gech,ehd->gecd', expert_hidden, w_exp_down, preferred_element...  4.18 us
    all_to_all x1, blocking collectives, local(): lax.all_to_all(attended, 'tp', split_axis=1, concat_axis=0, tiled=True)  3.79 us
    all_to_all x1, starting transfers between devices, sent_together(): lax.all_to_all(both, axis, split_axis=split_dim, concat_axis=concat_dim,...  3.68 us
    dot_general x1, matrix products, attend(): jnp.einsum('shc,spc->shp', query_latent, latents, preferred_element_type=...  3.54 us
  transfers between devices with their start and end apart: 4, of which 4 were waited for; matrix products, arithmetic and copies ran while one was open for 1% of the time, Pallas kernels for 0%

commit v1 on v0

--- a/solution.py
+++ b/solution.py
@@ -1,6 +1,8 @@
 import jax
 import jax.numpy as jnp
 from jax import lax
+from jax.experimental import pallas as pl
+from jax.experimental.pallas import tpu as pltpu
 from jax.sharding import PartitionSpec as P
 
 rms_eps = 1e-06
@@ -51,17 +53,6 @@
             axis=along,
         )
     )
-
-
-def cut_along(array, dim, size):
-    before, after = (array.shape[:dim], array.shape[dim + 1 :])
-    return jnp.moveaxis(array.reshape(*before, size, -1, *after), dim, 0)
-
-
-def summed_on_arrival(array, axis, dim):
-    size = lax.axis_size(axis)
-    blocks = lax.all_to_all(cut_along(array, dim, size), axis, 0, 0, tiled=True)
-    return jnp.sum(blocks, axis=0)
 
 
 def rms_scale(values, gain_vector):
@@ -87,24 +78,6 @@
     )
 
 
-def slot_tables(group_routes, group_weights, experts, capacity):
-    row_count, top_count = group_routes.shape
-    flat_routes = group_routes.reshape(-1)
-    matches = (flat_routes[:, None] == jnp.arange(experts, dtype=jnp.int32)[None, :]).astype(
-        jnp.int32
-    )
-    earlier = jnp.cumsum(matches, axis=0) - matches
-    slot_index = jnp.sum(earlier * matches, axis=1)
-    target = flat_routes * capacity + slot_index
-    slot_match = (
-        target[:, None] == jnp.arange(experts * capacity, dtype=jnp.int32)[None, :]
-    ).astype(jnp.float32)
-    slot_match = slot_match.reshape(row_count, top_count, experts * capacity)
-    dispatch = jnp.sum(slot_match, axis=1).T
-    weighing = jnp.sum(slot_match * group_weights[:, :, None], axis=1)
-    return (dispatch, weighing)
-
-
 def attend(query_latent, query_rope, latents, rope_keys, fresh_latent, fresh_rope, own_lengths):
     past_scores = jnp.einsum(
         "shc,spc->shp", query_latent, latents, preferred_element_type=jnp.float32
@@ -136,17 +109,382 @@
     return mixed_latent.astype(jnp.bfloat16)
 
 
-def expert_pass(expert_rows, w_exp_gate, w_exp_up, w_exp_down):
-    gate_value = jnp.einsum(
-        "gecd,edh->gech", expert_rows, w_exp_gate, preferred_element_type=jnp.float32
-    )
-    up_value = jnp.einsum(
-        "gecd,edh->gech", expert_rows, w_exp_up, preferred_element_type=jnp.float32
-    )
-    expert_hidden = (jax.nn.silu(gate_value) * up_value).astype(jnp.bfloat16)
-    return jnp.einsum(
-        "gech,ehd->gecd", expert_hidden, w_exp_down, preferred_element_type=jnp.float32
-    )
+mesh_ids = pl.DeviceIdType.MESH
+plane_size = 16
+group_rows = 16
+
+
+def remote(src, dst, send_sem, recv_sem, chip, core):
+    return pltpu.make_async_remote_copy(
+        src_ref=src,
+        dst_ref=dst,
+        send_sem=send_sem,
+        recv_sem=recv_sem,
+        device_id={"ep": chip, "tp": core},
+        device_id_type=mesh_ids,
+    )
+
+
+def rows_at(index):
+    return pl.ds(pl.multiple_of(index * group_rows, group_rows), group_rows)
+
+
+def half_at(core, width):
+    return pl.ds(pl.multiple_of(core * width, width), width)
+
+
+def greet(depth):
+    me, core = lax.axis_index("ep"), lax.axis_index("tp")
+    layer, spot = me // plane_size, lax.rem(me, plane_size)
+    barrier = pltpu.get_barrier_semaphore()
+
+    def signal(chip, to_core):
+        pl.semaphore_signal(
+            barrier, inc=1, device_id={"ep": chip, "tp": to_core}, device_id_type=mesh_ids
+        )
+
+    signal(me, 1 - core)
+
+    def in_column(k, carry):
+        signal(lax.rem(layer + k, depth) * plane_size + spot, core)
+        return carry
+
+    def in_plane(k, carry):
+        chip = layer * plane_size + lax.rem(spot + k, plane_size)
+        signal(chip, core)
+        signal(chip, 1 - core)
+        return carry
+
+    lax.fori_loop(1, depth, in_column, 0)
+    lax.fori_loop(1, plane_size, in_plane, 0)
+    pl.semaphore_wait(barrier, 1 + (depth - 1) + 2 * (plane_size - 1))
+
+
+def place_routes(routes_ref, weights_ref, table_buf, layer, depth):
+    lanes = lax.broadcasted_iota(jnp.int32, (routes_ref.shape[0], depth * group_rows), 1)
+    own = lanes // group_rows == layer
+    spread = jnp.concatenate([routes_ref[...].astype(jnp.float32)] * depth, axis=1)
+    spread_weights = jnp.concatenate([weights_ref[...]] * depth, axis=1)
+    top_count = routes_ref.shape[0]
+    table_buf[layer] = jnp.zeros(table_buf.shape[1:], jnp.float32)
+    table_buf[layer, 0:top_count] = jnp.where(own, spread, 0.0)
+    table_buf[layer, 8 : 8 + top_count] = jnp.where(own, spread_weights, 0.0)
+
+
+def tables(table_buf, layer, top_count):
+    table = jnp.sum(table_buf[...], axis=0)
+    token_count = table.shape[1]
+    shape = (plane_size * group_rows, token_count)
+    rows = lax.broadcasted_iota(jnp.int32, shape, 0)
+    lanes = lax.broadcasted_iota(jnp.int32, shape, 1)
+    expert = (layer * plane_size + rows // group_rows).astype(jnp.float32)
+    hit = jnp.zeros(shape, jnp.float32)
+    weight = jnp.zeros(shape, jnp.float32)
+    for k in range(top_count):
+        named = expert == table[k : k + 1]
+        hit = jnp.where(named, 1.0, hit)
+        weight = jnp.where(named, table[8 + k : 9 + k], weight)
+    same_group = lanes // group_rows == lax.rem(rows, group_rows) // 2
+    hit = jnp.where(same_group, hit, 0.0)
+    square = (token_count, token_count)
+    before = lax.broadcasted_iota(jnp.int32, square, 0) < lax.broadcasted_iota(
+        jnp.int32, square, 1
+    )
+    earlier = jnp.dot(
+        hit.astype(jnp.bfloat16),
+        jnp.where(before, 1.0, 0.0).astype(jnp.bfloat16),
+        preferred_element_type=jnp.float32,
+    )
+    chosen = (hit > 0.5) & (earlier == lax.rem(rows, 2).astype(jnp.float32))
+    dispatch = jnp.where(chosen, 1.0, 0.0).astype(jnp.bfloat16)
+    weighing = jnp.where(chosen, weight, 0.0).T.astype(jnp.bfloat16)
+    return dispatch, weighing
+
+
+def send_in_column(buf, slot_shape_at, send_sems, recv_sems, depth, source=None):
+    me, core = lax.axis_index("ep"), lax.axis_index("tp")
+    layer, spot = me // plane_size, lax.rem(me, plane_size)
+    for k in (4, 3, 5, 2, 6, 1, 7):
+        peer = lax.rem(layer + k, depth)
+        src = slot_shape_at(buf, layer) if source is None else slot_shape_at(source, peer)
+        remote(
+            src,
+            slot_shape_at(buf, layer),
+            send_sems.at[k],
+            recv_sems.at[layer],
+            peer * plane_size + spot,
+            core,
+        ).start()
+
+
+def column_waits(buf, slot_shape_at, send_sems, recv_sems, depth, sends):
+    me, core = lax.axis_index("ep"), lax.axis_index("tp")
+    layer, spot = me // plane_size, lax.rem(me, plane_size)
+    for k in (1, 7, 2, 6, 3, 5, 4):
+        peer = lax.rem(layer + k, depth)
+        copy = remote(
+            slot_shape_at(buf, peer),
+            slot_shape_at(buf, peer),
+            send_sems.at[k],
+            recv_sems.at[peer],
+            peer * plane_size + spot,
+            core,
+        )
+        if sends:
+            copy.wait_send()
+        else:
+            copy.wait_recv()
+
+
+def moe_kernel(
+    x_ref,
+    hidden_ref,
+    routes_ref,
+    weights_ref,
+    gate_hbm,
+    up_hbm,
+    down_hbm,
+    out_ref,
+    gate,
+    up,
+    down,
+    table_buf,
+    x_buf,
+    d_send,
+    r_buf,
+    y_send,
+    y_buf,
+    p_send,
+    p_buf,
+    load_sems,
+    w_send,
+    w_recv,
+    t_send,
+    t_recv,
+    x_send_sem,
+    x_recv,
+    d_send_sem,
+    d_recv,
+    y_send_sem,
+    y_recv,
+    p_send_sem,
+    p_recv,
+):
+    depth = table_buf.shape[0]
+    me, core = lax.axis_index("ep"), lax.axis_index("tp")
+    layer, spot = me // plane_size, lax.rem(me, plane_size)
+    half = x_ref.shape[1]
+    mine = lax.rem(spot, 2) == core
+    loads = [
+        pltpu.make_async_copy(src.at[0], dst.at[0], load_sems.at[n])
+        for n, (src, dst) in enumerate(((gate_hbm, gate), (up_hbm, up), (down_hbm, down)))
+    ]
+    for load in loads:
+        load.start()
+    place_routes(routes_ref, weights_ref, table_buf, layer, depth)
+    x_buf[rows_at(layer)] = x_ref[...]
+    greet(depth)
+
+    def tile_at(buf, slot):
+        return buf.at[slot]
+
+    def block_at(buf, slot):
+        return buf.at[rows_at(slot)]
+
+    send_in_column(table_buf, tile_at, t_send, t_recv, depth)
+    send_in_column(x_buf, block_at, x_send_sem, x_recv, depth)
+    swaps = [
+        remote(src.at[0], dst.at[1], w_send.at[n], w_recv.at[n], me, 1 - core)
+        for n, (src, dst) in enumerate(((gate_hbm, gate), (up_hbm, up), (down_hbm, down)))
+    ]
+    for swap in swaps:
+        swap.start()
+    column_waits(table_buf, tile_at, t_send, t_recv, depth, False)
+    dispatch, weighing = tables(table_buf, layer, routes_ref.shape[0])
+    column_waits(x_buf, block_at, x_send_sem, x_recv, depth, False)
+    d_send[...] = jnp.dot(dispatch, x_buf[...], preferred_element_type=jnp.float32).astype(
+        jnp.bfloat16
+    )
+
+    def row_copy(spot_to, spot_from, core_from):
+        return remote(
+            d_send.at[rows_at(spot_to)],
+            r_buf.at[rows_at(spot_from // 2), half_at(core_from, half)],
+            d_send_sem.at[spot_to],
+            d_recv.at[spot_from // 2, core_from],
+            layer * plane_size + spot_to,
+            lax.rem(spot_from, 2),
+        )
+
+    def send_rows(n, carry):
+        spot_to = spot ^ (15 - n)
+
+        @pl.when((spot_to != spot) | jnp.logical_not(mine))
+        def _():
+            row_copy(spot_to, spot, core).start()
+
+        return carry
+
+    lax.fori_loop(0, plane_size, send_rows, 0)
+
+    @pl.when(mine)
+    def _():
+        r_buf[rows_at(spot // 2), half_at(core, half)] = d_send[rows_at(spot)]
+
+    def recv_rows(n, carry):
+        spot_from = spot ^ (2 * (n // 2) + (lax.rem(spot, 2) ^ core))
+        core_from = lax.rem(n, 2)
+
+        @pl.when((spot_from != spot) | (core_from != core))
+        def _():
+            remote(
+                d_send.at[rows_at(0)],
+                r_buf.at[rows_at(spot_from // 2), half_at(core_from, half)],
+                d_send_sem.at[0],
+                d_recv.at[spot_from // 2, core_from],
+                me,
+                1 - core,
+            ).wait_recv()
+
+        return carry
+
+    lax.fori_loop(0, plane_size, recv_rows, 0)
+    for load in loads:
+        load.wait()
+    for swap in swaps:
+        swap.wait_recv()
+    rows = r_buf[...]
+    total = None
+    for part in range(2):
+        gate_value = jnp.dot(rows, gate[part], preferred_element_type=jnp.float32)
+        up_value = jnp.dot(rows, up[part], preferred_element_type=jnp.float32)
+        expert_hidden = (gate_value * jax.nn.sigmoid(gate_value) * up_value).astype(jnp.bfloat16)
+        term = jnp.dot(expert_hidden, down[part], preferred_element_type=jnp.float32)
+        total = term if total is None else total + term
+    y_send[...] = total.astype(jnp.bfloat16)
+
+    def back_copy(spot_to, core_to, spot_from):
+        return remote(
+            y_send.at[rows_at(spot_to // 2), half_at(core_to, half)],
+            y_buf.at[rows_at(spot_from)],
+            y_send_sem.at[spot_to // 2, core_to],
+            y_recv.at[spot_from],
+            layer * plane_size + spot_to,
+            core_to,
+        )
+
+    def send_back(n, carry):
+        spot_to = spot ^ (2 * (7 - n // 2) + (lax.rem(spot, 2) ^ core))
+        core_to = lax.rem(n, 2)
+
+        @pl.when((spot_to != spot) | (core_to != core))
+        def _():
+            back_copy(spot_to, core_to, spot).start()
+
+        return carry
+
+    lax.fori_loop(0, plane_size, send_back, 0)
+
+    @pl.when(mine)
+    def _():
+        y_buf[rows_at(spot)] = y_send[rows_at(spot // 2), half_at(core, half)]
+
+    def recv_back(n, carry):
+        spot_from = spot ^ n
+
+        @pl.when((spot_from != spot) | jnp.logical_not(mine))
+        def _():
+            remote(
+                y_send.at[rows_at(0), half_at(0, half)],
+                y_buf.at[rows_at(spot_from)],
+                y_send_sem.at[0, 0],
+                y_recv.at[spot_from],
+                me,
+                1 - core,
+            ).wait_recv()
+
+        return carry
+
+    lax.fori_loop(0, plane_size, recv_back, 0)
+    p_send[...] = jnp.dot(weighing, y_buf[...], preferred_element_type=jnp.float32).astype(
+        jnp.bfloat16
+    )
+    send_in_column(p_buf, block_at, p_send_sem, p_recv, depth, p_send)
+    p_buf[rows_at(layer)] = p_send[rows_at(layer)]
+    column_waits(p_buf, block_at, p_send_sem, p_recv, depth, False)
+    result = hidden_ref[...].astype(jnp.float32)
+    for n in range(depth):
+        result = result + p_buf[n * group_rows : (n + 1) * group_rows].astype(jnp.float32)
+    out_ref[...] = result.astype(jnp.bfloat16)
+
+    column_waits(table_buf, tile_at, t_send, t_recv, depth, True)
+    column_waits(x_buf, block_at, x_send_sem, x_recv, depth, True)
+    column_waits(p_buf, block_at, p_send_sem, p_recv, depth, True)
+    for swap in swaps:
+        swap.wait_send()
+
+    def sent_rows(n, carry):
+        @pl.when((n != spot) | jnp.logical_not(mine))
+        def _():
+            row_copy(n, spot, core).wait_send()
+
+        return carry
+
+    def sent_back(n, carry):
+        spot_to = 2 * (n // 2) + core
+        core_to = lax.rem(n, 2)
+
+        @pl.when((spot_to != spot) | (core_to != core))
+        def _():
+            back_copy(spot_to, core_to, spot).wait_send()
+
+        return carry
+
+    lax.fori_loop(0, plane_size, sent_rows, 0)
+    lax.fori_loop(0, plane_size, sent_back, 0)
+
+
+def routed_experts(x_half, own_half, routes, route_weights, w_exp_gate, w_exp_up, w_exp_down):
+    depth = lax.axis_size("ep") // plane_size
+    half = x_half.shape[1]
+    vmem = pl.BlockSpec(memory_space=pltpu.VMEM)
+    anywhere = pl.BlockSpec(memory_space=pl.ANY)
+    bf16, dma = jnp.bfloat16, pltpu.SemaphoreType.DMA
+    rows = plane_size * group_rows
+    hidden_half = w_exp_gate.shape[2]
+    return pl.pallas_call(
+        moe_kernel,
+        out_shape=jax.ShapeDtypeStruct(own_half.shape, bf16),
+        in_specs=[vmem] * 4 + [anywhere] * 3,
+        out_specs=vmem,
+        scratch_shapes=[
+            pltpu.VMEM((2, 2 * half, hidden_half), bf16),
+            pltpu.VMEM((2, 2 * half, hidden_half), bf16),
+            pltpu.VMEM((2, hidden_half, 2 * half), bf16),
+            pltpu.VMEM((depth, 16, depth * group_rows), jnp.float32),
+            pltpu.VMEM((depth * group_rows, half), bf16),
+            pltpu.VMEM((rows, half), bf16),
+            pltpu.VMEM((rows // 2, 2 * half), bf16),
+            pltpu.VMEM((rows // 2, 2 * half), bf16),
+            pltpu.VMEM((rows, half), bf16),
+            pltpu.VMEM((depth * group_rows, half), bf16),
+            pltpu.VMEM((depth * group_rows, half), bf16),
+            dma((3,)),
+            dma((3,)),
+            dma((3,)),
+            dma((depth,)),
+            dma((depth,)),
+            dma((depth,)),
+            dma((depth,)),
+            dma((plane_size,)),
+            dma((plane_size // 2, 2)),
+            dma((plane_size // 2, 2)),
+            dma((plane_size,)),
+            dma((depth,)),
+            dma((depth,)),
+        ],
+        compiler_params=pltpu.CompilerParams(collective_id=0, has_side_effects=True),
+    )(x_half, own_half, routes.T, route_weights.T, w_exp_gate, w_exp_up, w_exp_down)
 
 
 def local(
@@ -222,31 +560,11 @@
     )
     hidden1 = (token_values + attention_sum).astype(jnp.bfloat16)
     normed2 = rms_scale(hidden1.astype(jnp.float32), norm2_gain).astype(jnp.bfloat16)
-    own_half = lax.dynamic_slice_in_dim(hidden1, core_index * half_width, half_width, 1).astype(
-        jnp.float32
-    )
-    groups = lax.axis_size("ep")
-    experts_here = w_exp_gate.shape[0]
-    total_experts = groups * experts_here
-    top_count = routes.shape[1]
-    capacity = max(2, group_rows * top_count * 8 // 3 // total_experts)
-    dispatch, weighing = slot_tables(routes, route_weights, total_experts, capacity)
-    sent_rows = jnp.dot(
-        dispatch.astype(jnp.bfloat16), normed2, preferred_element_type=jnp.float32
-    ).astype(jnp.bfloat16)
-    sent_rows = sent_rows.reshape(groups, experts_here, capacity, model_width)
-    partial_out = expert_pass(
-        lax.all_to_all(sent_rows, "ep", split_axis=0, concat_axis=0, tiled=True),
-        w_exp_gate,
-        w_exp_up,
-        w_exp_down,
-    )
-    summed = summed_on_arrival(partial_out, "tp", 3).astype(jnp.bfloat16)
-    returned = lax.all_to_all(summed, "ep", split_axis=0, concat_axis=0, tiled=True)
-    routed = jnp.dot(
-        weighing, returned.reshape(total_experts * capacity, half_width).astype(jnp.float32)
-    )
-    mixed = (own_half + routed).astype(jnp.bfloat16)
+    own_half = lax.dynamic_slice_in_dim(hidden1, core_index * half_width, half_width, 1)
+    normed2_half = lax.dynamic_slice_in_dim(normed2, core_index * half_width, half_width, 1)
+    mixed = routed_experts(
+        normed2_half, own_half, routes, route_weights, w_exp_gate, w_exp_up, w_exp_down
+    )
     return (mixed, new_latent, new_rope_key)
 
 

time: 133 us -> 93.3 us (0.70)
  blocking collectives: 80.3 us -> 7.72 us
  Pallas kernels: 0 us -> 46.4 us
  matrix products: 16 us -> 12.1 us
  starting transfers between devices: 17.6 us -> 13.8 us
  local copies, waits for them, and re-layouts: 9.15 us -> 5.43 us
    all_to_all x3 -> x1, blocking collectives: 76.5 us -> 3.93 us  [from_everyone(): lax.all_to_all(jnp.broadcast_to(array[None], (size, *array.shape)), axis,...]
    pallas_call x0 -> x1, Pallas kernels: none -> 46.4 us  [routed_experts(): pl.pallas_call(moe_kernel, out_shape=jax.ShapeDtypeStruct(own_half.shape,...]
    dot_general x4 -> x0, matrix products: 6.18 us -> none  [the longest x1 4.18 us: expert_pass(): jnp.einsum('gech,ehd->gecd', expert_hidden, w_exp_down, preferred_element...]
    all_to_all x3 -> x2, starting transfers between devices: 13.9 us -> 10.2 us  [from_everyone(): lax.all_to_all(jnp.broadcast_to(array[None], (size, *array.shape)), axis,...]
    reshape x3 -> x0, local copies, waits for them, and re-layouts: 3.44 us -> none  [the longest x1 1.73 us: cut_along(): return jnp.moveaxis(array.reshape(*before, size, -1, *after), dim, 0)]
    reduce_sum x3 -> x0, other arithmetic: 2.09 us -> none  [the longest x1 1.82 us: summed_on_arrival(): return jnp.sum(blocks, axis=0)]
  transfers between devices with their start and end apart: 4 -> 3, of which waited for: 4 -> 3; matrix products, arithmetic and copies ran while one was open for 1% -> 0% of each run, Pallas kernels for 0% -> 0%
where the time goes in v1:
time: 93.3 us; the launch traced here: 92.5 us
  Pallas kernels  46.4 us (50%)
  starting transfers between devices  13.8 us (15%)
  matrix products  12.1 us (13%)
  blocking collectives  7.72 us (8%)
  local copies, waits for them, and re-layouts  5.43 us (6%)
  waiting for transfers between devices  3.24 us (3%)
  other arithmetic  2.88 us (3%)
    pallas_call x1, Pallas kernels, routed_experts(): pl.pallas_call(moe_kernel, out_shape=jax.ShapeDtypeStruct(own_half.shape,...  46.4 us
    all_to_all x2, starting transfers between devices, from_everyone(): lax.all_to_all(jnp.broadcast_to(array[None], (size, *array.shape)), axis,...  10.2 us
    all_to_all x1, blocking collectives, from_everyone(): lax.all_to_all(jnp.broadcast_to(array[None], (size, *array.shape)), axis,...  3.93 us
    all_to_all x1, blocking collectives, local(): lax.all_to_all(attended, 'tp', split_axis=1, concat_axis=0, tiled=True)  3.79 us
    dot_general x1, matrix products, attend(): jnp.einsum('shc,spc->shp', query_latent, latents, preferred_element_type=...  3.69 us
    all_to_all x1, starting transfers between devices, sent_together(): lax.all_to_all(both, axis, split_axis=split_dim, concat_axis=concat_dim,...  3.68 us
    broadcast_in_dim x3, local copies, waits for them, and re-layouts, from_everyone(): jnp.broadcast_to(array[None], (size, *array.shape))  2.24 us
    all_to_all x2, waiting for transfers between devices, from_everyone(): lax.all_to_all(jnp.broadcast_to(array[None], (size, *array.shape)), axis,...  2.15 us
  transfers between devices with their start and end apart: 3, of which 3 were waited for; matrix products, arithmetic and copies ran while one was open for 0% of the time, Pallas kernels for 0%

profile of v1, /device:TPU:1, one launch (start us, length us, event | category | flops | bytes accessed | tf_op | source)
XLA Modules:
  0.0 92.5 jit_solution(5665746361411926279)
XLA Ops:
  0.7 1.5 %broadcast_in_dim.9 = bf16[2,16,1024]{2,1,0:T(8,128)(2,1)} broadcast(bf16[16,1024]{1,0:T(8,128)(2,1)} %param.21), dimensions={1,2} | broadcast | bytes 98304 | tf_op jit(solution)/shard_map/broadcast_in_dim | solution.py:21
  2.2 6.5 %all-to-all-start = ((bf16[2,16,1024]{2,1,0:T(8,128)(2,1)}), bf16[2,16,1024]{2,1,0:T(8,128)(2,1)S(1)}, u32[]{:S(2)}, u32[]{:S(2)}) async-start(bf16[2,16,1024]{2,1,0:T(8,128)(2,1)} %broadcast_in_dim.9), calls=%async_computation | async-start | bytes 131072 | tf_op jit(solution)/shard_map/all_to_all | solution.py:20
  8.7 1.1 %all-to-all-done = bf16[2,16,1024]{2,1,0:T(8,128)(2,1)S(1)} async-done(((bf16[2,16,1024]{2,1,0:T(8,128)(2,1)}), bf16[2,16,1024]{2,1,0:T(8,128)(2,1)S(1)}, u32[]{:S(2)}, u32[]{:S(2)}) %all-to-all-start) | async-done | bytes 65568 | tf_op jit(solution)/shard_map/all_to_all | solution.py:20
  9.9 0.7 dynamic-slice
  10.7 1.5 %convolution_bitcast_fusion.1 = f32[2,4,8,128]{3,2,1,0:T(8,128)S(1)} fusion(bf16[16,1024]{1,0:T(8,128)(2,1)S(1)} %fusion.13, bf16[1024,512]{1,0:T(8,128)(2,1)} %param.26), kind=kOutput, calls=%fused_computation.11 | convolution fusion | flops 16777216 | bytes 1114112 | tf_op jit(solution)/shard_map/dot_general | solution.py:526
  12.2 1.2 %convolution_bitcast_fusion.2 = f32[2,2,8,128]{3,2,1,0:T(8,128)S(1)} fusion(bf16[16,1024]{1,0:T(8,128)(2,1)S(1)} %fusion.13, bf16[1024,256]{1,0:T(8,128)(2,1)} %param.27), kind=kOutput, calls=%fused_computation.12 | convolution fusion | flops 8388608 | bytes 573440 | tf_op jit(solution)/shard_map/dot_general | solution.py:527
  13.4 1.0 %fusion.40 = f32[16,32]{1,0:T(8,128)S(1)} fusion(bf16[16,1024]{1,0:T(8,128)(2,1)S(1)} %fusion.13, bf16[1024,32]{0,1:T(8,128)(2,1)} %param.28), kind=kOutput, calls=%fused_computation.76 | convolution fusion | flops 1048576 | bytes 100352 | tf_op jit(solution)/shard_map/dot_general | solution.py:528
  14.5 0.7 broadcast_in_dim.10
  15.2 3.7 %all-to-all-start.1 = ((f32[2,1,12800]{2,1,0:T(1,128)}), f32[2,1,12800]{2,1,0:T(1,128)S(1)}, u32[]{:S(2)}, u32[]{:S(2)}) async-start(f32[2,1,12800]{2,1,0:T(1,128)} %broadcast_in_dim.10), calls=%async_computation.1 | async-start | bytes 204800 | tf_op jit(solution)/shard_map/all_to_all | solution.py:20
  18.9 1.1 %all-to-all-done.1 = f32[2,1,12800]{2,1,0:T(1,128)S(1)} async-done(((f32[2,1,12800]{2,1,0:T(1,128)}), f32[2,1,12800]{2,1,0:T(1,128)S(1)}, u32[]{:S(2)}, u32[]{:S(2)}) %all-to-all-start.1) | async-done | bytes 102432 | tf_op jit(solution)/shard_map/all_to_all | solution.py:20
  20.2 0.7 convert_element_type.85
  21.0 1.3 %fusion.32 = f32[16,8,32]{2,0,1:T(8,128)S(1)} fusion(bf16[512,8,32]{0,2,1:T(8,128)(2,1)} %param.32, f32[16,512]{1,0:T(8,128)S(1)} %slice.50, f32[512]{0:T(512)} %param.29, f32[16]{0:T(128)S(1)} %add_rsqrt_fusion.2), kind=kOutput, calls=%fused_computation.72 | convolution fusion | flops 4218880 | bytes 313408 | tf_op jit(solution)/shard_map/sc,chd->shd/dot_general | solution.py:538
  22.3 1.6 %fusion.3 = bf16[16,8,256]{2,0,1:T(8,128)(2,1)S(1)} fusion(bf16[8,64,256]{2,1,0:T(8,128)(2,1)} %param.33, bf16[512,8,64]{0,2,1:T(8,128)(2,1)} %param.31, f32[16,512]{1,0:T(8,128)S(1)} %slice.50, f32[512]{0:T(512)} %param.29, f32[16]{0:T(128)S(1)} %add_rsqrt_fusion.2), kind=kOutput, calls=%fused_computation.7 | convolution fusion | flops 12681216 | bytes 886848 | tf_op jit(solution)/shard_map/shd,hdc->shc/dot_general | solution.py:543
  24.2 0.6 copy.51
  24.9 3.7 %all-to-all-start.2 = ((bf16[16,8,288]{2,1,0:T(8,128)(2,1)}), bf16[16,8,288]{2,1,0:T(8,128)(2,1)S(1)}, u32[]{:S(2)}, u32[]{:S(2)}) async-start(bf16[16,8,288]{2,1,0:T(8,128)(2,1)} %copy.51), calls=%async_computation.2 | async-start | bytes 196608 | tf_op jit(solution)/shard_map/all_to_all | solution.py:51
  28.6 1.1 %all-to-all-done.2 = bf16[16,8,288]{2,1,0:T(8,128)(2,1)S(1)} async-done(((bf16[16,8,288]{2,1,0:T(8,128)(2,1)}), bf16[16,8,288]{2,1,0:T(8,128)(2,1)S(1)}, u32[]{:S(2)}, u32[]{:S(2)}) %all-to-all-start.2) | async-done | bytes 73760 | tf_op jit(solution)/shard_map/all_to_all | solution.py:51
  30.4 3.7 %fusion.19 = f32[8,16,1024]{2,1,0:T(8,128)S(1)} fusion(bf16[8,1024,256]{2,1,0:T(8,128)(2,1)} %param.23, bf16[8,16,288]{2,1,0:T(8,128)(2,1)S(1)} %bitcast.76), kind=kOutput, calls=%fused_computation.40 | convolution fusion | flops 67108864 | bytes 4784128 | tf_op jit(solution)/shard_map/shc,spc->shp/dot_general | solution.py:82
  34.7 0.7 fusion.2
  35.4 3.8 %all_to_all.52 = bf16[8,16,256]{2,0,1:T(8,128)(2,1)S(1)} all-to-all(bf16[8,16,256]{2,0,1:T(8,128)(2,1)S(1)} %copy.53), channel_id=1, replica_groups=mesh['ep'=128,'tp'=2] {'tp'}, dimensions={1} | all-to-all | bytes 131072 | tf_op jit(solution)/shard_map/all_to_all | solution.py:554
  39.3 0.6 convolution_bitcast_fusion
  39.9 3.9 %all_to_all.53 = f32[2,16,2048]{2,1,0:T(8,128)S(1)} all-to-all(f32[2,16,2048]{2,1,0:T(8,128)S(1)} %broadcast_in_dim.12), channel_id=1, replica_groups=mesh['ep'=128,'tp'=2] {'tp'}, dimensions={0} | all-to-all | bytes 524288 | tf_op jit(solution)/shard_map/all_to_all | solution.py:20
  44.0 0.7 multiply_convert_fusion
  44.7 46.4 %shard_map.220 = bf16[16,1024]{1,0:T(8,128)(2,1)} custom-call(bf16[16,1024]{1,0:T(8,128)(2,1)} %get-tuple-element.3.x_ref, bf16[16,1024]{1,0:T(8,128)(2,1)} %get-tuple-element.4.hidden_ref, s32[6,16]{1,0:T(8,128)} %bitcast.83, f32[6,16]{1,0:T(8,128)} %bitcast.84, bf16[1,2048,256]{2,1,0:T(8,128)(2,1)} %gate_hbm.1, bf16[1,2048,256]{2,1,0:T(8,128)(2,1)} %up_hbm.1, ...), custom_call_target="tpu_custom_call" | custom-call | tf_op jit(solution)/shard_map/pallas_call | solution.py:455
  91.1 1.4 %copy.84 = bf16[16,1024]{1,0:T(8,128)(2,1)} copy(bf16[16,1024]{1,0:T(8,128)(2,1)} %shard_map.220) | data formatting | bytes 65536
  (61 shorter events, 2.6 us)
Async XLA Ops:
  0.6 38.6 %copy-start = (bf16[8,64,2048]{2,1,0:T(8,128)(2,1)S(1)}, bf16[8,64,2048]{2,1,0:T(8,128)(2,1)}, u32[]{:S(2)}) copy-start(bf16[8,64,2048]{2,1,0:T(8,128)(2,1)} %param.35) | copy-start | bytes 6291460
  0.6 29.1 %copy-start.7 = (s32[16]{0:T(128)S(1)}, s32[16]{0:T(128)}, u32[]{:S(2)}) copy-start(s32[16]{0:T(128)} %param.22) | copy-start | bytes 196
  0.7 29.5 %copy-start.6 = (f32[256]{0:T(256)S(1)}, f32[256]{0:T(256)}, u32[]{:S(2)}) copy-start(f32[256]{0:T(256)} %param.30) | copy-start | bytes 3076
  2.2 7.6 %all-to-all-start = ((bf16[2,16,1024]{2,1,0:T(8,128)(2,1)}), bf16[2,16,1024]{2,1,0:T(8,128)(2,1)S(1)}, u32[]{:S(2)}, u32[]{:S(2)}) async-start(bf16[2,16,1024]{2,1,0:T(8,128)(2,1)} %broadcast_in_dim.9), calls=%async_computation | async-start | bytes 131072 | tf_op jit(solution)/shard_map/all_to_all | solution.py:20
  14.5 19.6 %copy-start.2 = (bf16[8,1024,32]{1,2,0:T(8,128)(2,1)S(1)}, bf16[8,1024,32]{1,2,0:T(8,128)(2,1)}, u32[]{:S(2)}) copy-start(bf16[8,1024,32]{1,2,0:T(8,128)(2,1)} %param.24) | copy-start | bytes 1572868
  15.2 4.8 %all-to-all-start.1 = ((f32[2,1,12800]{2,1,0:T(1,128)}), f32[2,1,12800]{2,1,0:T(1,128)S(1)}, u32[]{:S(2)}, u32[]{:S(2)}) async-start(f32[2,1,12800]{2,1,0:T(1,128)} %broadcast_in_dim.10), calls=%async_computation.1 | async-start | bytes 204800 | tf_op jit(solution)/shard_map/all_to_all | solution.py:20
  24.9 4.8 %all-to-all-start.2 = ((bf16[16,8,288]{2,1,0:T(8,128)(2,1)}), bf16[16,8,288]{2,1,0:T(8,128)(2,1)S(1)}, u32[]{:S(2)}, u32[]{:S(2)}) async-start(bf16[16,8,288]{2,1,0:T(8,128)(2,1)} %copy.51), calls=%async_computation.2 | async-start | bytes 196608 | tf_op jit(solution)/shard_map/all_to_all | solution.py:51
  29.8 4.8 %copy-start.1 = (bf16[8,1024,256]{2,1,0:T(8,128)(2,1)S(1)}, bf16[8,1024,256]{2,1,0:T(8,128)(2,1)}, u32[]{:S(2)}) copy-start(bf16[8,1024,256]{2,1,0:T(8,128)(2,1)} %param.23) | copy-start | bytes 12582916
  30.0 5.3 %copy-start.5 = (bf16[8,32]{1,0:T(8,128)(2,1)}, bf16[8,32]{1,0:T(8,128)(2,1)S(1)}, u32[]{:S(2)}) copy-start(bf16[8,32]{1,0:T(8,128)(2,1)S(1)} %fusion.30) | copy-start | bytes 1540
  30.2 5.1 %copy-start.4 = (bf16[8,256]{1,0:T(8,128)(2,1)}, bf16[8,256]{1,0:T(8,128)(2,1)S(1)}, u32[]{:S(2)}) copy-start(bf16[8,256]{1,0:T(8,128)(2,1)S(1)} %get-tuple-element.23) | copy-start | bytes 12292
  34.1 5.2 %copy-start.3 = (bf16[8,256,64]{1,2,0:T(8,128)(2,1)S(1)}, bf16[8,256,64]{1,2,0:T(8,128)(2,1)}, u32[]{:S(2)}) copy-start(bf16[8,256,64]{1,2,0:T(8,128)(2,1)} %param.34) | copy-start | bytes 786436
  34.6 9.3 %dynamic-slice-start = ((f32[2048]{0:T(1024)}, s32[]{:T(128)}), f32[1024]{0:T(1024)S(1)}, s32[]{:S(2)}) async-start(f32[2048]{0:T(1024)} %param.36, s32[]{:T(128)} %select_n.15), calls=%async_computation.5 | async-start | bytes 8704 | tf_op jit(solution)/shard_map/dynamic_slice | solution.py:564
